TPU v7x, 32 devices: a whole 2x2x4 slice. The times are simulated.
32 devices in a mesh: ep: 8 (over z, y), tp: 4 (over x, core).
Axes of the slice: x: 2, y: 2, z: 4, core: 2. Of those that a mesh axis runs over, the one named last changes fastest.
Arguments:
- tokens: bfloat16 [1344, 2048], P('ep'), may hold values from -6 to 6
- cotangent: bfloat16 [1344, 2048], P('ep'), may hold values from -6 to 6
- group_ids: int32 [1344, 1], P('ep'), may hold values from 0 to 7; in each aligned block of 168 rows (0 to 167, 168 to 335, ...) at most 32 rows name the same one
- within_ids: int32 [1344, 2], P('ep'), may hold values from 0 to 1, all different within a row
- gate_weights: bfloat16 [1344, 2], P('ep'), may hold values from 0.099609375 to 1
- w_gate: bfloat16 [16, 2048, 1024], P('ep', None, 'tp'), may hold values from -0.125 to 0.125
- w_up: bfloat16 [16, 2048, 1024], P('ep', None, 'tp'), may hold values from -0.125 to 0.125
- w_down: bfloat16 [16, 1024, 2048], P('ep', 'tp'), may hold values from -0.1875 to 0.1875
Outputs:
- tokens_grad: bfloat16 [1344, 2048], P('ep', 'tp')
- gate_grad: float32 [1344, 2], P('ep')
- w_gate_grad: bfloat16 [16, 2048, 1024], P('ep', None, 'tp')
- w_up_grad: bfloat16 [16, 2048, 1024], P('ep', None, 'tp')
- w_down_grad: bfloat16 [16, 1024, 2048], P('ep', 'tp')
Inputs may be any that keep to these rules, and one draw needn't show every extreme that they name: `group_ids`: in the rows of one device no group is chosen by more than 32 rows. `within_ids`: the two entries of a row differ.
All inputs are finite; a program needn't handle non-finite values.
Results may differ from a plain program's by a relative error of at most 0.017.
Values may be sent and summed in bfloat16 or wider, within the bound.
A program may use at most 64 MiB of HBM per device.

v0:
```python
import functools

import jax
import jax.numpy as jnp
from jax import lax
from jax.experimental import pallas as pl
from jax.experimental.pallas import tpu as pltpu
from jax.sharding import PartitionSpec as P

MESH = pl.DeviceIdType.MESH
LANES = 128
NT = (((1,), (1,)), ((), ()))
TN = (((0,), (0,)), ((), ()))
NN = (((1,), (0,)), ((), ()))


def dot(a, b, dims=NN):
    return lax.dot_general(a, b, dims, preferred_element_type=jnp.float32)


def each(count, body):
    if count <= 8:
        for i in range(count):
            body(i)
    else:
        lax.fori_loop(0, count, lambda i, c: (body(i), c)[1], 0)


def aligned(value, step):
    return value if isinstance(value, int) else pl.multiple_of(value, step)


def kernel(
    ep, tp, cap,
    tok_ref, cot_ref, gid_ref, wid_ref, gw_ref, wg_ref, wu_ref, wd_ref,
    place_ref, back, gate_back, vwg, vwu, vwd,
    src, placed, rows_in, wg, wu, wd, acc, gate_b, up_b, act_c,
    to_partner, from_partner, dx_acc, to_x, from_x, to_ep,
    gate_in, gate_sum,
    load_sem, own_sem, send1, recv_rows, send_x, send_p, send_p2,
    dxp_send, dxp_recv, dxx_send, dxx_recv, dxe_send, dxe_recv,
    gt_send, gt_recv, ge_send, ge_recv,
):
    e_me = lax.axis_index("ep")
    t_me = lax.axis_index("tp")
    core = lax.rem(t_me, 2)
    x_me = lax.div(t_me, 2)
    partner = t_me + 1 - 2 * core
    nx = tp // 2
    gate_lanes = gate_back.shape[2]
    tok_rows, width = tok_ref.shape
    cs = width // tp
    slots = ep * cap
    experts = wg.shape[0]
    bf16 = jnp.bfloat16

    barrier = pltpu.get_barrier_semaphore()
    each(ep - 1, lambda i: pl.semaphore_signal(
        barrier, inc=1, device_id=(lax.rem(e_me + 1 + i, ep), t_me), device_id_type=MESH))
    each(tp - 1, lambda i: pl.semaphore_signal(
        barrier, inc=1, device_id=(e_me, lax.rem(t_me + 1 + i, tp)), device_id_type=MESH))

    my_cols = pl.ds(pl.multiple_of(t_me * cs, LANES), cs)
    loads = [
        pltpu.make_async_copy(tok_ref.at[:, my_cols], src.at[:, pl.ds(0, cs)], load_sem.at[0]),
        pltpu.make_async_copy(cot_ref.at[:, my_cols], src.at[:, pl.ds(cs, cs)], load_sem.at[1]),
        pltpu.make_async_copy(wg_ref, wg, load_sem.at[2]),
        pltpu.make_async_copy(wu_ref, wu, load_sem.at[3]),
        pltpu.make_async_copy(wd_ref, wd, load_sem.at[4]),
    ]
    for load in loads[:2]:
        load.start()

    group = gid_ref[...]
    groups = -(-ep // 16) * 16
    in_group = (
        lax.broadcasted_iota(jnp.int32, (groups, tok_rows), 0) == group
    ).astype(jnp.float32)
    earlier = (
        lax.broadcasted_iota(jnp.int32, (tok_rows, tok_rows), 0)
        < lax.broadcasted_iota(jnp.int32, (tok_rows, tok_rows), 1)
    ).astype(jnp.float32).astype(bf16)
    before = dot(in_group.astype(bf16), earlier)
    rank = jnp.sum(before * in_group, axis=0, keepdims=True).astype(jnp.int32)
    slot_row = lax.broadcasted_iota(jnp.int32, (slots, tok_rows), 0)
    place = (slot_row == group * cap + rank).astype(jnp.float32).astype(bf16)
    place_ref[0] = place
    place_ref[1] = (slot_row == e_me * cap % gate_lanes + rank).astype(jnp.float32).astype(bf16)
    lane_row = lax.broadcasted_iota(jnp.int32, (LANES, tok_rows), 0)
    weights = gw_ref[...].astype(jnp.float32)
    comb = jnp.zeros((LANES, tok_rows), jnp.float32)
    for k in range(weights.shape[0]):
        comb = comb + jnp.where(lane_row == wid_ref[k : k + 1, :], weights[k : k + 1, :], 0.0)
    placed[:, pl.ds(2 * cs, LANES)] = dot(place, comb.astype(bf16), NT).astype(bf16)
    loads[0].wait()
    placed[:, pl.ds(0, cs)] = dot(place, src[:, pl.ds(0, cs)]).astype(bf16)
    loads[1].wait()
    for load in loads[2:]:
        load.start()
    placed[:, pl.ds(cs, cs)] = dot(place, src[:, pl.ds(cs, cs)]).astype(bf16)

    pl.semaphore_wait(barrier, ep + tp - 2)

    def xor(d):
        value, bit = 0, 1
        while bit < ep:
            value = value + (e_me // bit + d // bit) % 2 * bit
            bit *= 2
        return value

    def target(d):
        return xor(d) if ep & (ep - 1) == 0 else lax.rem(e_me + d, ep)

    def source(d):
        return xor(d) if ep & (ep - 1) == 0 else lax.rem(e_me - d + ep, ep)

    def block(e):
        return pl.ds(aligned(e * cap, 16), cap)

    distances = list(range(ep))
    def stage1(d):
        g = target(d)
        return pltpu.make_async_remote_copy(
            src_ref=placed.at[block(g)], dst_ref=rows_in.at[t_me, block(e_me)],
            send_sem=send1.at[d], recv_sem=recv_rows.at[t_me, e_me],
            device_id=(g, t_me), device_id_type=MESH)

    own = pltpu.make_async_copy(
        placed.at[block(e_me)], rows_in.at[t_me, block(e_me)], own_sem.at[0])
    own.start()
    if ep <= 8:
        for d in distances[1:]:
            stage1(d).start()
    else:
        each(ep - 1, lambda i: stage1(i + 1).start())

    def arrived(q, e, cols):
        part = rows_in.at[q, block(e), pl.ds(0, cols)]
        pltpu.make_async_remote_copy(
            src_ref=part, dst_ref=part, send_sem=send1.at[0], recv_sem=recv_rows.at[q, e],
            device_id=(e_me, partner), device_id_type=MESH).wait_recv()

    def forward(q, e, sem, target):
        part = rows_in.at[q, block(e), pl.ds(0, 2 * cs)]
        return pltpu.make_async_remote_copy(
            src_ref=part, dst_ref=part, send_sem=sem, recv_sem=recv_rows.at[q, e],
            device_id=(e_me, target), device_id_type=MESH)

    def x_peer(k):
        return lax.rem(x_me + k, nx) * 2 + core

    def to_peers(d):
        e = source(d)
        copies = [forward(t_me, e, send_x.at[k - 1, d], x_peer(k)) for k in range(1, nx)]
        return copies + [forward(t_me, e, send_p.at[d], partner)]

    def stage2(d):
        for copy in to_peers(d):
            copy.start()

    def relays(d):
        e = source(d)
        return [(x_peer(k), e, forward(x_peer(k), e, send_p2.at[k - 1, d], partner))
                for k in range(1, nx)]

    def stage3(d):
        for q, e, copy in relays(d):
            arrived(q, e, 2 * cs)
            copy.start()

    own.wait()
    stage2(0)
    if ep <= 8:
        for i, d in enumerate(distances[1:]):
            arrived(t_me, source(d), 2 * cs + LANES)
            stage2(d)
    else:
        def later(i):
            arrived(t_me, source(i + 1), 2 * cs + LANES)
            stage2(i + 1)
        each(ep - 1, later)

    for load in loads[2:]:
        load.wait()

    def share(q):
        return pl.ds(aligned(q * cs, LANES), cs)

    def hidden(q, first):
        xq = rows_in[q, :, pl.ds(0, cs)]
        yq = rows_in[q, :, pl.ds(cs, cs)]
        for e in range(experts):
            for n, value in enumerate((
                dot(xq, wg[e, share(q), :]),
                dot(xq, wu[e, share(q), :]),
                dot(yq, wd[e, :, share(q)], NT),
            )):
                acc[e, n] = value if first else acc[e, n] + value

    def all_arrived(q):
        each(ep, lambda e: arrived(q, e, 2 * cs))

    hidden(t_me, True)
    if ep <= 8:
        for d in distances:
            stage3(d)
    else:
        each(ep, stage3)
    all_arrived(partner)
    hidden(partner, False)

    def x_quarters(k):
        hidden(x_peer(k), False)
        other = lax.rem(x_me + k, nx) * 2 + 1 - core
        all_arrived(other)
        hidden(other, False)
    each(nx - 1, lambda i: x_quarters(i + 1))

    row8 = lax.broadcasted_iota(jnp.int32, (8, slots), 0)
    gates = jnp.zeros((8, slots), jnp.float32)
    for e in range(experts):
        pre_gate, pre_up, dy_down = acc[e, 0], acc[e, 1], acc[e, 2]
        c = rows_in[t_me, :, pl.ds(2 * cs, LANES)][:, e : e + 1].astype(jnp.float32)
        sig = jax.nn.sigmoid(pre_gate)
        silu = pre_gate * sig
        act = silu * pre_up
        prod = act.astype(bf16).astype(jnp.float32) * dy_down
        act_grad = c * dy_down
        act_c[e] = (c * act).astype(bf16)
        gate_b[e] = (act_grad * pre_up * sig * (1.0 + pre_gate * (1.0 - sig))).astype(bf16)
        up_b[e] = (act_grad * silu).astype(bf16)
        high = prod.astype(bf16)
        low = (prod - high.astype(jnp.float32)).astype(bf16)
        ones = jnp.ones((8, prod.shape[1]), bf16)
        gates = gates + jnp.where(row8 == e, dot(ones, high, NT) + dot(ones, low, NT), 0.0)
    gate_in[t_me] = gates

    def gate_tp(i):
        return pltpu.make_async_remote_copy(
            src_ref=gate_in.at[t_me], dst_ref=gate_in.at[t_me],
            send_sem=gt_send.at[i], recv_sem=gt_recv.at[t_me],
            device_id=(e_me, lax.rem(t_me + 1 + i, tp)), device_id_type=MESH)

    def dx_of(q):
        total = None
        for e in range(experts):
            part = dot(gate_b[e], wg[e, share(q), :], NT) + dot(up_b[e], wu[e, share(q), :], NT)
            total = part if total is None else total + part
        return total

    def dx_partner(k):
        return pltpu.make_async_remote_copy(
            src_ref=to_partner.at[k], dst_ref=from_partner.at[k],
            send_sem=dxp_send.at[k], recv_sem=dxp_recv.at[k],
            device_id=(e_me, partner), device_id_type=MESH)

    def give_partner(i):
        k = nx - 1 - i
        to_partner[k] = dx_of(lax.rem(x_me + k, nx) * 2 + 1 - core).astype(bf16)
        dx_partner(k).start()

    def dx_x(k, d):
        e = target(d)
        return pltpu.make_async_remote_copy(
            src_ref=to_x.at[k - 1, block(e)], dst_ref=from_x.at[k - 1, block(e)],
            send_sem=dxx_send.at[k - 1, d], recv_sem=dxx_recv.at[k - 1, d],
            device_id=(e_me, x_peer(k)), device_id_type=MESH)

    far = distances[::-1]

    def walk(body):
        if ep <= 8:
            for i, d in enumerate(far):
                body(i, d)
        else:
            each(ep, lambda i: body(i, ep - 1 - i))

    def give_x(k):
        mine = dx_of(x_peer(k))
        dx_partner(k).wait_recv()
        to_x[k - 1] = (mine + from_partner[k].astype(jnp.float32)).astype(bf16)
        walk(lambda i, d: dx_x(k, d).start())
    each(tp - 1, lambda i: gate_tp(i).start())

    def cross(i):
        give_partner(i)
        give_x(nx - 1 - i)
    each(nx - 1, cross)
    give_partner(nx - 1)
    mine = dx_of(t_me)
    dx_partner(0).wait_recv()
    dx_acc[...] = mine + from_partner[0].astype(jnp.float32)

    def gate_tile(e):
        return pl.ds(pl.multiple_of(e * cap // gate_lanes * gate_lanes, LANES), gate_lanes)

    def gate_ep(d):
        return pltpu.make_async_remote_copy(
            src_ref=gate_sum.at[:, gate_tile(target(d))], dst_ref=gate_back.at[e_me],
            send_sem=ge_send.at[d], recv_sem=ge_recv.at[e_me],
            device_id=(target(d), t_me), device_id_type=MESH)

    def gate_wait(i):
        q = lax.rem(t_me + 1 + i, tp)
        pltpu.make_async_remote_copy(
            src_ref=gate_in.at[q], dst_ref=gate_in.at[q],
            send_sem=gt_send.at[i], recv_sem=gt_recv.at[q],
            device_id=(e_me, q), device_id_type=MESH).wait_recv()

    def gates_on():
        each(tp - 1, gate_wait)
        total = gate_in[0]
        for q in range(1, tp):
            total = total + gate_in[q]
        gate_sum[...] = total
        gate_back[e_me] = gate_sum[:, gate_tile(e_me)]
        each(ep - 1, lambda i: gate_ep(i + 1).start())

    def weight_grads(q):
        x_t = rows_in[q, :, pl.ds(0, cs)].T
        yq = rows_in[q, :, pl.ds(cs, cs)]
        for e in range(experts):
            vwg[e, share(q), :] = dot(x_t, gate_b[e]).astype(bf16)
            vwu[e, share(q), :] = dot(x_t, up_b[e]).astype(bf16)
            vwd[e, :, share(q)] = dot(act_c[e], yq, TN).astype(bf16)

    def dx_ep(d):
        g = target(d)
        return pltpu.make_async_remote_copy(
            src_ref=to_ep.at[block(g)], dst_ref=back.at[block(e_me)],
            send_sem=dxe_send.at[d], recv_sem=dxe_recv.at[e_me],
            device_id=(g, t_me), device_id_type=MESH)

    def finish_chunk(d):
        rows = block(target(d))
        value = dx_acc[rows, :]
        for k in range(1, nx):
            dx_x(k, d).wait_recv()
            value = value + from_x[k - 1, rows, :].astype(jnp.float32)
        return value.astype(bf16)

    def chunk(i, d):
        to_ep[block(target(d)), :] = finish_chunk(d)
        dx_ep(d).start()

    if ep <= 8:
        done = 0
        for i, d in enumerate(far[:-1]):
            chunk(i, d)
            if i % 2 == 0 and done < tp:
                weight_grads(done)
                done += 1
            if i == min(2, ep - 2):
                gates_on()
        for q in range(done, tp):
            weight_grads(q)
    else:
        each(ep - 1, lambda i: chunk(i, ep - 1 - i))
        each(tp, weight_grads)
        gates_on()
    back[block(e_me), :] = finish_chunk(0)

    def gate_arrived(i):
        g = lax.rem(e_me + 1 + i, ep)
        pltpu.make_async_remote_copy(
            src_ref=gate_sum.at[:, gate_tile(g)], dst_ref=gate_back.at[g],
            send_sem=ge_send.at[0], recv_sem=ge_recv.at[g],
            device_id=(g, t_me), device_id_type=MESH).wait_recv()
    each(ep - 1, gate_arrived)
    def back_arrived(i):
        g = lax.rem(e_me + 1 + i, ep)
        pltpu.make_async_remote_copy(
            src_ref=to_ep.at[block(g)], dst_ref=back.at[block(g)],
            send_sem=dxe_send.at[0], recv_sem=dxe_recv.at[g],
            device_id=(g, t_me), device_id_type=MESH).wait_recv()
    each(ep - 1, back_arrived)

    def sent1(i):
        d = i + 1
        stage1(d).wait_send()
        gate_ep(d).wait_send()
        dx_ep(d).wait_send()
    each(ep - 1, sent1)

    def sent2(d):
        for copy in to_peers(d):
            copy.wait_send()
        for _, _, copy in relays(d):
            copy.wait_send()
        for k in range(1, nx):
            dx_x(k, d).wait_send()
    each(ep, sent2)
    each(nx, lambda k: dx_partner(k).wait_send())
    each(tp - 1, lambda i: gate_tp(i).wait_send())


def finish(
    place_ref, back, gate_back, vwg, vwu, vwd, gid_ref, wid_ref,
    dtok_ref, dgate_ref, gwg_ref, gwu_ref, gwd_ref, dtok, dgate, sem,
):
    copies = []
    for a, b in ((vwg, gwg_ref), (vwu, gwu_ref), (vwd, gwd_ref)):
        experts, rows, _ = a.shape
        for e in range(experts):
            for half in range(2):
                part = pl.ds(half * (rows // 2), rows // 2)
                copies.append(pltpu.make_async_copy(
                    a.at[e, part], b.at[e, part], sem.at[2 + len(copies)]))
    for copy in copies:
        copy.start()
    ep, _, slots = gate_back.shape
    tok_rows = place_ref.shape[2]
    dtok[...] = dot(place_ref[0], back[...], TN).astype(jnp.bfloat16)
    copies.append(pltpu.make_async_copy(dtok, dtok_ref, sem.at[0]))
    copies[-1].start()
    sums = gate_back[...].reshape(ep * 8, slots)
    high = sums.astype(jnp.bfloat16)
    low = (sums - high.astype(jnp.float32)).astype(jnp.bfloat16)
    pick = place_ref[1, :slots, :]
    dense = dot(high, pick) + dot(low, pick)
    row = lax.broadcasted_iota(jnp.int32, (ep * 8, tok_rows), 0)
    for k in range(wid_ref.shape[0]):
        wanted = row == gid_ref[...] * 8 + wid_ref[k : k + 1, :]
        dgate[k : k + 1, :] = jnp.sum(jnp.where(wanted, dense, 0.0), axis=0, keepdims=True)
    copies.append(pltpu.make_async_copy(dgate, dgate_ref, sem.at[1]))
    copies[-1].start()
    for copy in copies:
        copy.wait()


def on_device(tokens, cotangent, group_ids, within_ids, gate_weights, w_gate, w_up, w_down):
    ep = lax.axis_size("ep")
    tp = lax.axis_size("tp")
    tok_rows, width = tokens.shape
    experts, _, ff = w_gate.shape
    cap = (3 * tok_rows + 2 * ep - 1) // (2 * ep)
    cap = -(-cap // 16) * 16
    slots = ep * cap
    gate_lanes = LANES if LANES % cap == 0 and slots % LANES == 0 else slots
    cs = width // tp
    nx = tp // 2
    bf16, f32 = jnp.bfloat16, jnp.float32
    dma = pltpu.SemaphoreType.DMA
    hbm = pl.BlockSpec(memory_space=pltpu.HBM)
    vmem = pl.BlockSpec(memory_space=pltpu.VMEM)
    scratch = [
        pltpu.VMEM((tok_rows, 2 * cs), bf16),
        pltpu.VMEM((slots, 2 * cs + LANES), bf16),
        pltpu.VMEM((tp, slots, 2 * cs + LANES), bf16),
        pltpu.VMEM(w_gate.shape, bf16),
        pltpu.VMEM(w_up.shape, bf16),
        pltpu.VMEM(w_down.shape, bf16),
        pltpu.VMEM((experts, 3, slots, ff), f32),
        pltpu.VMEM((experts, slots, ff), bf16),
        pltpu.VMEM((experts, slots, ff), bf16),
        pltpu.VMEM((experts, slots, ff), bf16),
        pltpu.VMEM((nx, slots, cs), bf16),
        pltpu.VMEM((nx, slots, cs), bf16),
        pltpu.VMEM((slots, cs), f32),
        pltpu.VMEM((nx - 1, slots, cs), bf16),
        pltpu.VMEM((nx - 1, slots, cs), bf16),
        pltpu.VMEM((slots, cs), bf16),
        pltpu.VMEM((tp, 8, slots), f32),
        pltpu.VMEM((8, slots), f32),
        dma((5,)), dma((1,)), dma((ep,)), dma((tp, ep)),
        dma((nx - 1, ep)), dma((ep,)), dma((nx - 1, ep)),
        dma((nx,)), dma((nx,)), dma((nx - 1, ep)), dma((nx - 1, ep)), dma((ep,)), dma((ep,)),
        dma((tp,)), dma((tp,)), dma((ep,)), dma((ep,)),
    ]
    gid, wid, gw = group_ids.T, within_ids.T, gate_weights.T
    kept = pl.pallas_call(
        functools.partial(kernel, ep, tp, cap),
        out_shape=(
            pltpu.VMEM((2, slots, tok_rows), bf16),
            pltpu.VMEM((slots, cs), bf16),
            pltpu.VMEM((ep, 8, gate_lanes), f32),
            pltpu.VMEM(w_gate.shape, bf16),
            pltpu.VMEM(w_up.shape, bf16),
            pltpu.VMEM(w_down.shape, bf16),
        ),
        in_specs=[hbm, hbm, vmem, vmem, vmem, hbm, hbm, hbm],
        out_specs=(vmem,) * 6,
        scratch_shapes=scratch,
        compiler_params=pltpu.CompilerParams(
            collective_id=0, has_side_effects=True, vmem_limit_bytes=57 * 1024 * 1024),
    )(tokens, cotangent, gid, wid, gw, w_gate, w_up, w_down)
    dtok, dgate, gwg, gwu, gwd = pl.pallas_call(
        finish,
        out_shape=(
            jax.ShapeDtypeStruct((tok_rows, cs), bf16),
            jax.ShapeDtypeStruct(wid.shape, f32),
            jax.ShapeDtypeStruct(w_gate.shape, bf16),
            jax.ShapeDtypeStruct(w_up.shape, bf16),
            jax.ShapeDtypeStruct(w_down.shape, bf16),
        ),
        in_specs=[vmem] * 8,
        out_specs=(hbm,) * 5,
        scratch_shapes=[
            pltpu.VMEM((tok_rows, cs), bf16),
            pltpu.VMEM(wid.shape, f32),
            dma((2 + 6 * experts,)),
        ],
        compiler_params=pltpu.CompilerParams(vmem_limit_bytes=12 * 1024 * 1024),
    )(*kept, gid, wid)
    return dtok, dgate.T, gwg, gwu, gwd


def solution(mesh):
    in_specs = (
        P("ep", None),
        P("ep", None),
        P("ep", None),
        P("ep", None),
        P("ep", None),
        P("ep", None, "tp"),
        P("ep", None, "tp"),
        P("ep", "tp", None),
    )
    out_specs = (
        P("ep", "tp"),
        P("ep", None),
        P("ep", None, "tp"),
        P("ep", None, "tp"),
        P("ep", "tp", None),
    )
    return jax.shard_map(
        on_device, mesh=mesh, in_specs=in_specs, out_specs=out_specs, check_vma=False
    )
```

profile of v0, /device:TPU:0, one launch (start us, length us, event | category | flops | bytes accessed | tf_op | source)
XLA Modules:
  0.0 44.0 jit_solution(17925269628753032345)
XLA Ops:
  0.6 0.0 copy-start
  0.6 0.0 copy-start.1
  0.7 40.5 %shard_map.119 = (bf16[2,256,168]{2,1,0:T(8,128)(2,1)S(1)}, bf16[256,512]{1,0:T(8,128)(2,1)S(1)}, f32[8,8,128]{2,1,0:T(8,128)S(1)}, bf16[2,2048,256]{2,1,0:T(8,1...) custom-call(bf16[168,2048]{1,0:T(8,128)(2,1)} %tok_ref.1, bf16[168,2048]{1,0:T(8,128)(2,1)} %cot_ref.1, ...), custom_call_target="tpu_custom_call" | custom-call | tf_op jit(solution)/shard_map/pallas_call | solution.py:471
  41.1 0.0 copy-done
  41.2 0.0 copy-done.1
  41.2 2.8 %shard_map.120 = (bf16[168,512]{1,0:T(8,128)(2,1)}, f32[2,168]{1,0:T(2,128)}, bf16[2,2048,256]{2,1,0:T(8,128)(2,1)}, bf16[2,2048,256]{2,1,0:T(8,128)(2,1)}, bf16[2,256,2048]{2,1,0:T(8,128)(2,1)}) custom-call(bf16[2,256,168]{2,1,0:T(8,128)(2,1)S(1)} %get-tuple-element.16.place_ref, bf16[256,512]{1,0:T(8,128)(2,1)S(1)} %get-tuple-element.17.back, ...), custom_call_target="tpu_custom_call" | custom-call | tf_op jit(solution)/shard_map/pallas_call | solution.py:487
Async XLA Ops:
  0.6 40.5 %copy-start = (s32[168,2]{0,1:T(2,128)S(1)}, s32[168,2]{0,1:T(2,128)}, u32[]{:S(2)}) copy-start(s32[168,2]{0,1:T(2,128)} %param.11) | copy-start | bytes 4036
  0.6 40.5 %copy-start.1 = (s32[168,1]{0,1:T(1,128)S(1)}, s32[168,1]{0,1:T(1,128)}, u32[]{:S(2)}) copy-start(s32[168,1]{0,1:T(1,128)} %param.10) | copy-start | bytes 2020
where the time goes:
time: 44.1 us; the launch traced here: 44 us
  Pallas kernels  43.3 us (98%)
  between operations  0.67 us (2%)
    pallas_call x1, Pallas kernels, on_device(): pl.pallas_call(functools.partial(kernel, ep, tp, cap), out_shape=(pltpu.V...  40.5 us
    pallas_call x1, Pallas kernels, on_device(): pl.pallas_call(finish, out_shape=(jax.ShapeDtypeStruct((tok_rows, cs), bf...  2.82 us

commit v1 on v0

--- a/solution.py
+++ b/solution.py
@@ -394,6 +394,410 @@
     each(tp - 1, lambda i: gate_tp(i).wait_send())
 
 
+def fast_kernel(
+    ep, tp, cap,
+    tok_ref, cot_ref, gid_ref, wid_ref, gw_ref, wg_ref, wu_ref, wd_ref,
+    place_ref, back, gate_back, vwg, vwu, vwd,
+    gid, wid, gw, src, tok_all, cot_all, placed, rows_in, wg, wu, wd,
+    acc, gate_b, up_b, act_c, prod_hi, prod_lo, c_out, c_in,
+    to_partner, from_partner, dx_acc, dx_far, to_x, from_x, to_ep, gate_in, gate_sum,
+    load_sem, send1, recv_rows, send_p, send_x, send_r, c_send, c_recv,
+    dxp_send, dxp_recv, dxx_send, dxx_recv, dxe_send, dxe_recv,
+    gt_send, gt_recv, ge_send, ge_recv,
+):
+    e_me = lax.axis_index("ep")
+    t_me = lax.axis_index("tp")
+    core = lax.rem(t_me, 2)
+    x_me = lax.div(t_me, 2)
+    x_other = 1 - x_me
+    partner = 2 * x_me + 1 - core
+    cross = 2 * x_other + 1 - core
+    beyond = 2 * x_other + core
+    lanes = gate_back.shape[2]
+    tok_rows, width = tok_ref.shape
+    cs = width // tp
+    slots = ep * cap
+    experts = wg.shape[0]
+    bf16 = jnp.bfloat16
+
+    barrier = pltpu.get_barrier_semaphore()
+    for i in range(ep - 1):
+        pl.semaphore_signal(
+            barrier, inc=1, device_id=(lax.rem(e_me + 1 + i, ep), partner), device_id_type=MESH)
+    for i in range(tp - 1):
+        pl.semaphore_signal(
+            barrier, inc=1, device_id=(e_me, lax.rem(t_me + 1 + i, tp)), device_id_type=MESH)
+
+    my_cols = pl.ds(pl.multiple_of(t_me * cs, LANES), cs)
+    loads = [pltpu.make_async_copy(a, b, load_sem.at[i]) for i, (a, b) in enumerate((
+        (gid_ref, gid), (wid_ref, wid), (gw_ref, gw),
+        (tok_ref.at[:, my_cols], src.at[:, pl.ds(0, cs)]),
+        (cot_ref.at[:, my_cols], src.at[:, pl.ds(cs, cs)]),
+        (tok_ref, tok_all), (cot_ref, cot_all),
+        (wg_ref, wg), (wu_ref, wu), (wd_ref, wd),
+    ))]
+    for load in loads[:5]:
+        load.start()
+    earlier = (
+        lax.broadcasted_iota(jnp.int32, (tok_rows, tok_rows), 0)
+        < lax.broadcasted_iota(jnp.int32, (tok_rows, tok_rows), 1)
+    ).astype(jnp.float32).astype(bf16)
+    slot_row = lax.broadcasted_iota(jnp.int32, (slots, tok_rows), 0)
+    for load in loads[:3]:
+        load.wait()
+
+    group = gid[...]
+    groups = -(-ep // 16) * 16
+    in_group = (
+        lax.broadcasted_iota(jnp.int32, (groups, tok_rows), 0) == group
+    ).astype(jnp.float32)
+    before = dot(in_group.astype(bf16), earlier)
+    rank = jnp.sum(before * in_group, axis=0, keepdims=True).astype(jnp.int32)
+    place = (slot_row == group * cap + rank).astype(jnp.float32).astype(bf16)
+    place_ref[0] = place
+    loads[3].wait()
+    placed[:, pl.ds(0, cs)] = dot(place, src[:, pl.ds(0, cs)]).astype(bf16)
+    loads[4].wait()
+    placed[:, pl.ds(cs, cs)] = dot(place, src[:, pl.ds(cs, cs)]).astype(bf16)
+    for load in loads[5:]:
+        load.start()
+
+    def xor(d):
+        value, bit = 0, 1
+        while bit < ep:
+            value = value + (e_me // bit + d // bit) % 2 * bit
+            bit *= 2
+        return value
+
+    def block(e):
+        return pl.ds(aligned(e * cap, 16), cap)
+
+    def tile_of(e):
+        return e * cap // lanes
+
+    pl.semaphore_wait(barrier, ep + tp - 2)
+
+    def send_rows(d):
+        g = xor(d)
+        return pltpu.make_async_remote_copy(
+            src_ref=placed.at[block(g)], dst_ref=rows_in.at[t_me, block(e_me)],
+            send_sem=send1.at[d], recv_sem=recv_rows.at[t_me, e_me],
+            device_id=(g, partner), device_id_type=MESH)
+
+    def send_c(d):
+        g = xor(d)
+        return pltpu.make_async_remote_copy(
+            src_ref=c_out.at[tile_of(g)], dst_ref=c_in.at[e_me],
+            send_sem=c_send.at[d], recv_sem=c_recv.at[e_me],
+            device_id=(g, partner), device_id_type=MESH)
+
+    others = list(range(1, ep))
+    for d in others[ep // 2 - 2::-1] + others[:ep // 2 - 2:-1]:
+        send_rows(d).start()
+    lane_row = lax.broadcasted_iota(jnp.int32, (16, tok_rows), 0)
+    weights = gw[...].astype(jnp.float32)
+    comb = jnp.zeros((16, tok_rows), jnp.float32)
+    for k in range(weights.shape[0]):
+        comb = comb + jnp.where(lane_row == wid[k : k + 1, :], weights[k : k + 1, :], 0.0)
+    c_rows = dot(comb.astype(bf16), place, NT)
+    for i in range(slots // lanes):
+        c_out[i] = c_rows[:experts, i * lanes : (i + 1) * lanes]
+    for d in others:
+        send_c(d).start()
+
+    def arrived(q, d):
+        e = xor(d)
+        part = rows_in.at[q, block(e)]
+        pltpu.make_async_remote_copy(
+            src_ref=part, dst_ref=part, send_sem=send1.at[0], recv_sem=recv_rows.at[q, e],
+            device_id=(e_me, partner), device_id_type=MESH).wait_recv()
+
+    def pass_on(q, d, sem, device):
+        e = xor(d)
+        part = rows_in.at[q, block(e)]
+        return pltpu.make_async_remote_copy(
+            src_ref=part, dst_ref=part, send_sem=sem.at[d], recv_sem=recv_rows.at[q, e],
+            device_id=(e_me, device), device_id_type=MESH)
+
+    def to_chips(ds):
+        for d in ds:
+            arrived(partner, d)
+            pass_on(partner, d, send_x, cross).start()
+            pass_on(partner, d, send_p, partner).start()
+
+    def relay(ds):
+        for d in ds:
+            arrived(beyond, d)
+            pass_on(beyond, d, send_r, partner).start()
+
+    def wait_rows(q, ds):
+        for d in ds:
+            arrived(q, d)
+
+    loads[5].wait()
+    loads[6].wait()
+    own = place_ref[0, block(e_me), :]
+    own_x = dot(own, tok_all[...]).astype(bf16)
+    own_y = dot(own, cot_all[...]).astype(bf16)
+    for q in range(tp):
+        rows_in[q, block(e_me), pl.ds(0, cs)] = own_x[:, q * cs : (q + 1) * cs]
+        rows_in[q, block(e_me), pl.ds(cs, cs)] = own_y[:, q * cs : (q + 1) * cs]
+    c_in[e_me] = c_out[tile_of(e_me)]
+    place_ref[1] = (slot_row == e_me * cap % lanes + rank).astype(jnp.float32).astype(bf16)
+
+    def chunk_of(d, n):
+        first = xor(d)
+        first = first - lax.rem(first, n)
+        return first, n, pl.ds(pl.multiple_of(first * cap, cap), n * cap)
+
+    def share(q):
+        return pl.ds(aligned(q * cs, LANES), cs)
+
+    def lhs(x, rows, first):
+        return jnp.concatenate(
+            [rows_in[2 * x + i, rows, pl.ds(first, cs)] for i in range(2)], axis=1)
+
+    def half(chunk, x, keep):
+        rows = chunk[2]
+        xs, ys = lhs(x, rows, 0), lhs(x, rows, cs)
+        cols = pl.ds(pl.multiple_of(x * 2 * cs, LANES), 2 * cs)
+        out = []
+        for e in range(experts):
+            values = (dot(xs, wg[e, cols, :]), dot(xs, wu[e, cols, :]), dot(ys, wd[e, :, cols], NT))
+            if keep:
+                for n, value in enumerate(values):
+                    acc[e, n, rows, :] = value
+            out.append(values)
+        return out
+
+    def first_half(chunk):
+        half(chunk, x_me, True)
+
+    lane = lax.broadcasted_iota(jnp.int32, (cap, lanes), 1)
+    lane = lane - lax.broadcasted_iota(jnp.int32, (cap, lanes), 0)
+    my_lane = lane == lax.rem(e_me * cap, lanes)
+
+    def second_half(chunk):
+        first, n, rows = chunk
+        sums = half(chunk, x_other, False)
+        for e in range(experts):
+            pre_gate, pre_up, dy_down = (acc[e, m, rows, :] + sums[e][m] for m in range(3))
+            c = jnp.concatenate([
+                jnp.sum(jnp.where(my_lane, c_in[first + i, e : e + 1, :], 0.0), axis=1, keepdims=True)
+                for i in range(n)], axis=0)
+            sig = jax.nn.sigmoid(pre_gate)
+            silu = pre_gate * sig
+            act = silu * pre_up
+            prod = act.astype(bf16).astype(jnp.float32) * dy_down
+            act_grad = c * dy_down
+            act_c[e, rows, :] = (c * act).astype(bf16)
+            gate_b[e, rows, :] = (act_grad * pre_up * sig * (1.0 + pre_gate * (1.0 - sig))).astype(bf16)
+            up_b[e, rows, :] = (act_grad * silu).astype(bf16)
+            high = prod.astype(bf16)
+            prod_hi[e, rows, :] = high
+            prod_lo[e, rows, :] = (prod - high.astype(jnp.float32)).astype(bf16)
+
+    def dx_of(chunk, q, n):
+        rows, total = chunk[2], None
+        cols = pl.ds(pl.multiple_of(q * cs, LANES), n * cs)
+        for e in range(experts):
+            part = dot(gate_b[e, rows, :], wg[e, cols, :], NT)
+            part = part + dot(up_b[e, rows, :], wu[e, cols, :], NT)
+            total = part if total is None else total + part
+        return total
+
+    def dx_partner(k, i, chunk):
+        return pltpu.make_async_remote_copy(
+            src_ref=to_partner.at[k, chunk[2]], dst_ref=from_partner.at[k, chunk[2]],
+            send_sem=dxp_send.at[k, i], recv_sem=dxp_recv.at[k, i],
+            device_id=(e_me, partner), device_id_type=MESH)
+
+    def dx_x(d):
+        e = xor(d)
+        return pltpu.make_async_remote_copy(
+            src_ref=to_x.at[block(e)], dst_ref=from_x.at[block(e)],
+            send_sem=dxx_send.at[d], recv_sem=dxx_recv.at[d],
+            device_id=(e_me, cross), device_id_type=MESH)
+
+    def dx_first(i, chunk):
+        rows = chunk[2]
+        to_partner[0, rows, :] = dx_of(chunk, cross, 1).astype(bf16)
+        dx_partner(0, i, chunk).start()
+
+    def dx_rest(i, chunk):
+        rows = chunk[2]
+        dx_far[rows, :] = dx_of(chunk, beyond, 1)
+        both = dx_of(chunk, 2 * x_me, 2)
+        low, high = both[:, :cs], both[:, cs:]
+        to_partner[1, rows, :] = jnp.where(core == 0, low, high).astype(bf16)
+        dx_partner(1, i, chunk).start()
+        dx_acc[rows, :] = jnp.where(core == 0, high, low)
+
+    def dx_over(i, chunk, ds):
+        dx_partner(0, i, chunk).wait_recv()
+        for d in ds:
+            rows = block(xor(d))
+            to_x[rows, :] = (dx_far[rows, :] + from_partner[0, rows, :].astype(jnp.float32)).astype(bf16)
+            dx_x(d).start()
+
+    def dx_ep(d):
+        g = xor(d)
+        return pltpu.make_async_remote_copy(
+            src_ref=to_ep.at[block(g)], dst_ref=back.at[block(e_me)],
+            send_sem=dxe_send.at[d], recv_sem=dxe_recv.at[e_me],
+            device_id=(g, partner), device_id_type=MESH)
+
+    def own_ready(i, chunk):
+        dx_partner(1, i, chunk).wait_recv()
+
+    def send_back(ds):
+        for d in ds:
+            rows = block(xor(d))
+            dx_x(d).wait_recv()
+            value = dx_acc[rows, :] + from_partner[1, rows, :].astype(jnp.float32)
+            to_ep[rows, :] = (value + from_x[rows, :].astype(jnp.float32)).astype(bf16)
+            dx_ep(d).start()
+
+    def gate_tp(i):
+        return pltpu.make_async_remote_copy(
+            src_ref=gate_in.at[t_me], dst_ref=gate_in.at[t_me],
+            send_sem=gt_send.at[i], recv_sem=gt_recv.at[t_me],
+            device_id=(e_me, lax.rem(t_me + 1 + i, tp)), device_id_type=MESH)
+
+    def gate_ep(d):
+        g = xor(d)
+        return pltpu.make_async_remote_copy(
+            src_ref=gate_sum.at[tile_of(g)], dst_ref=gate_back.at[e_me],
+            send_sem=ge_send.at[d], recv_sem=ge_recv.at[e_me],
+            device_id=(g, partner), device_id_type=MESH)
+
+    def gates():
+        row8 = lax.broadcasted_iota(jnp.int32, (8, slots), 0)
+        ones = jnp.ones((8, prod_hi.shape[2]), bf16)
+        value = jnp.zeros((8, slots), jnp.float32)
+        for e in range(experts):
+            total = dot(ones, prod_hi[e], NT) + dot(ones, prod_lo[e], NT)
+            value = value + jnp.where(row8 == e, total, 0.0)
+        gate_in[t_me] = value[:experts]
+        for i in range(tp - 1):
+            gate_tp(i).start()
+
+    def gates_on():
+        for i in range(tp - 1):
+            q = lax.rem(t_me + 1 + i, tp)
+            pltpu.make_async_remote_copy(
+                src_ref=gate_in.at[q], dst_ref=gate_in.at[q],
+                send_sem=gt_send.at[i], recv_sem=gt_recv.at[q],
+                device_id=(e_me, q), device_id_type=MESH).wait_recv()
+        total = gate_in[0]
+        for q in range(1, tp):
+            total = total + gate_in[q]
+        for i in range(slots // lanes):
+            gate_sum[i] = total[:, i * lanes : (i + 1) * lanes]
+        gate_back[e_me] = gate_sum[tile_of(e_me)]
+        for d in others:
+            gate_ep(d).start()
+
+    def weight_grads(q):
+        x_t = rows_in[q, :, pl.ds(0, cs)].T
+        yq = rows_in[q, :, pl.ds(cs, cs)]
+        for e in range(experts):
+            vwg[e, share(q), :] = dot(x_t, gate_b[e]).astype(bf16)
+            vwu[e, share(q), :] = dot(x_t, up_b[e]).astype(bf16)
+            vwd[e, :, share(q)] = dot(act_c[e], yq, TN).astype(bf16)
+
+    near = others[ep // 2 - 2::-1]
+    far_b = others[:-1 - ep // 4:-1]
+    far_c = others[-1 - ep // 4:ep // 2 - 2:-1]
+    far = far_b + far_c
+    a, f = chunk_of(0, ep // 2), chunk_of(ep // 2, ep // 2)
+    b, c = chunk_of(far_b[0], ep // 4), chunk_of(far_c[0], ep // 4)
+
+    def c_arrived(ds):
+        for d in ds:
+            e = xor(d)
+            pltpu.make_async_remote_copy(
+                src_ref=c_out.at[0], dst_ref=c_in.at[e], send_sem=c_send.at[0],
+                recv_sem=c_recv.at[e], device_id=(e_me, partner), device_id_type=MESH).wait_recv()
+
+    to_chips(near)
+    for load in loads[7:]:
+        load.wait()
+    wait_rows(t_me, near)
+    first_half(a)
+    to_chips(far_b)
+    relay(near)
+    wait_rows(cross, near)
+    c_arrived(near)
+    second_half(a)
+    to_chips(far_c[:1])
+    dx_first(0, a)
+    to_chips(far_c[1:])
+    relay(far_b)
+    dx_rest(0, a)
+    wait_rows(t_me, far)
+    first_half(f)
+    wait_rows(cross, far_b)
+    c_arrived(far)
+    second_half(b)
+    relay(far_c)
+    dx_first(1, b)
+    dx_rest(1, b)
+    dx_over(1, b, far_b)
+    dx_over(0, a, [0] + near)
+    wait_rows(cross, far_c)
+    second_half(c)
+    dx_first(2, c)
+    gates()
+    dx_rest(2, c)
+    dx_over(2, c, far_c)
+    own_ready(1, b)
+    send_back(far_b)
+    gates_on()
+    weight_grads(0)
+    own_ready(0, a)
+    own_ready(2, c)
+    send_back(far_c)
+    send_back(near + [0])
+    weight_grads(1)
+    weight_grads(2)
+    weight_grads(3)
+
+    def returned(d):
+        g = xor(d)
+        pltpu.make_async_remote_copy(
+            src_ref=gate_sum.at[0], dst_ref=gate_back.at[g],
+            send_sem=ge_send.at[0], recv_sem=ge_recv.at[g],
+            device_id=(g, partner), device_id_type=MESH).wait_recv()
+
+    def rows_back(d):
+        g = xor(d)
+        pltpu.make_async_remote_copy(
+            src_ref=to_ep.at[block(g)], dst_ref=back.at[block(g)],
+            send_sem=dxe_send.at[0], recv_sem=dxe_recv.at[g],
+            device_id=(g, partner), device_id_type=MESH).wait_recv()
+
+    for d in others:
+        returned(d)
+    for d in range(ep):
+        rows_back(d)
+    for d in range(ep):
+        dx_x(d).wait_send()
+        dx_ep(d).wait_send()
+    for d in others:
+        send_rows(d).wait_send()
+        send_c(d).wait_send()
+        pass_on(partner, d, send_x, cross).wait_send()
+        pass_on(partner, d, send_p, partner).wait_send()
+        pass_on(beyond, d, send_r, partner).wait_send()
+        gate_ep(d).wait_send()
+    for i, chunk in enumerate((a, b, c)):
+        for k in range(2):
+            dx_partner(k, i, chunk).wait_send()
+    for i in range(tp - 1):
+        gate_tp(i).wait_send()
+
+
 def finish(
     place_ref, back, gate_back, vwg, vwu, vwd, gid_ref, wid_ref,
     dtok_ref, dgate_ref, gwg_ref, gwu_ref, gwd_ref, dtok, dgate, sem,
@@ -408,19 +812,19 @@
                     a.at[e, part], b.at[e, part], sem.at[2 + len(copies)]))
     for copy in copies:
         copy.start()
-    ep, _, slots = gate_back.shape
+    ep, per, slots = gate_back.shape
     tok_rows = place_ref.shape[2]
     dtok[...] = dot(place_ref[0], back[...], TN).astype(jnp.bfloat16)
     copies.append(pltpu.make_async_copy(dtok, dtok_ref, sem.at[0]))
     copies[-1].start()
-    sums = gate_back[...].reshape(ep * 8, slots)
+    sums = jnp.concatenate([gate_back[e] for e in range(ep)], axis=0)
     high = sums.astype(jnp.bfloat16)
     low = (sums - high.astype(jnp.float32)).astype(jnp.bfloat16)
     pick = place_ref[1, :slots, :]
     dense = dot(high, pick) + dot(low, pick)
-    row = lax.broadcasted_iota(jnp.int32, (ep * 8, tok_rows), 0)
+    row = lax.broadcasted_iota(jnp.int32, (ep * per, tok_rows), 0)
     for k in range(wid_ref.shape[0]):
-        wanted = row == gid_ref[...] * 8 + wid_ref[k : k + 1, :]
+        wanted = row == gid_ref[...] * per + wid_ref[k : k + 1, :]
         dgate[k : k + 1, :] = jnp.sum(jnp.where(wanted, dense, 0.0), axis=0, keepdims=True)
     copies.append(pltpu.make_async_copy(dgate, dgate_ref, sem.at[1]))
     copies[-1].start()
@@ -468,17 +872,53 @@
         dma((tp,)), dma((tp,)), dma((ep,)), dma((ep,)),
     ]
     gid, wid, gw = group_ids.T, within_ids.T, gate_weights.T
+    body, per, small = kernel, 8, vmem
+    if ep == 8 and tp == 4 and gate_lanes == LANES:
+        body, per, small = fast_kernel, experts, hbm
+        scratch = [
+            pltpu.VMEM(gid.shape, jnp.int32),
+            pltpu.VMEM(wid.shape, jnp.int32),
+            pltpu.VMEM(gw.shape, bf16),
+            pltpu.VMEM((tok_rows, 2 * cs), bf16),
+            pltpu.VMEM((tok_rows, width), bf16),
+            pltpu.VMEM((tok_rows, width), bf16),
+            pltpu.VMEM((slots, 2 * cs), bf16),
+            pltpu.VMEM((tp, slots, 2 * cs), bf16),
+            pltpu.VMEM(w_gate.shape, bf16),
+            pltpu.VMEM(w_up.shape, bf16),
+            pltpu.VMEM(w_down.shape, bf16),
+            pltpu.VMEM((experts, 3, slots, ff), f32),
+            pltpu.VMEM((experts, slots, ff), bf16),
+            pltpu.VMEM((experts, slots, ff), bf16),
+            pltpu.VMEM((experts, slots, ff), bf16),
+            pltpu.VMEM((experts, slots, ff), bf16),
+            pltpu.VMEM((experts, slots, ff), bf16),
+            pltpu.VMEM((slots // gate_lanes, experts, gate_lanes), f32),
+            pltpu.VMEM((ep, experts, gate_lanes), f32),
+            pltpu.VMEM((2, slots, cs), bf16),
+            pltpu.VMEM((2, slots, cs), bf16),
+            pltpu.VMEM((slots, cs), f32),
+            pltpu.VMEM((slots, cs), f32),
+            pltpu.VMEM((slots, cs), bf16),
+            pltpu.VMEM((slots, cs), bf16),
+            pltpu.VMEM((slots, cs), bf16),
+            pltpu.VMEM((tp, experts, slots), f32),
+            pltpu.VMEM((slots // gate_lanes, experts, gate_lanes), f32),
+            dma((10,)), dma((ep,)), dma((tp, ep)), dma((ep,)), dma((ep,)), dma((ep,)),
+            dma((ep,)), dma((ep,)), dma((2, 3)), dma((2, 3)), dma((ep,)), dma((ep,)),
+            dma((ep,)), dma((ep,)), dma((tp,)), dma((tp,)), dma((ep,)), dma((ep,)),
+        ]
     kept = pl.pallas_call(
-        functools.partial(kernel, ep, tp, cap),
+        functools.partial(body, ep, tp, cap),
         out_shape=(
             pltpu.VMEM((2, slots, tok_rows), bf16),
             pltpu.VMEM((slots, cs), bf16),
-            pltpu.VMEM((ep, 8, gate_lanes), f32),
+            pltpu.VMEM((ep, per, gate_lanes), f32),
             pltpu.VMEM(w_gate.shape, bf16),
             pltpu.VMEM(w_up.shape, bf16),
             pltpu.VMEM(w_down.shape, bf16),
         ),
-        in_specs=[hbm, hbm, vmem, vmem, vmem, hbm, hbm, hbm],
+        in_specs=[hbm, hbm, small, small, small, hbm, hbm, hbm],
         out_specs=(vmem,) * 6,
         scratch_shapes=scratch,
         compiler_params=pltpu.CompilerParams(

time: 44.1 us -> 41.8 us (0.948)
  Pallas kernels: 43.3 us -> 40.9 us
    pallas_call x1, Pallas kernels: 40.5 us -> 38.1 us  [on_device(): pl.pallas_call(functools.partial(body, ep, tp, cap), out_shape=(pltpu.VME...]
where the time goes in v1:
time: 41.8 us; the launch traced here: 41.6 us
  Pallas kernels  40.9 us (98%)
  between operations  0.67 us (2%)
    pallas_call x1, Pallas kernels, on_device(): pl.pallas_call(functools.partial(body, ep, tp, cap), out_shape=(pltpu.VME...  38.1 us
    pallas_call x1, Pallas kernels, on_device(): pl.pallas_call(finish, out_shape=(jax.ShapeDtypeStruct((tok_rows, cs), bf...  2.82 us

profile of v1, /device:TPU:0, one launch (start us, length us, event | category | flops | bytes accessed | tf_op | source)
XLA Modules:
  0.0 41.6 jit_solution(10256043905136965047)
XLA Ops:
  0.6 0.0 copy-start
  0.6 0.0 copy-start.1
  0.7 38.1 %shard_map.119 = (bf16[2,256,168]{2,1,0:T(8,128)(2,1)S(1)}, bf16[256,512]{1,0:T(8,128)(2,1)S(1)}, f32[8,2,128]{2,1,0:T(2,128)S(1)}, bf16[2,2048,256]{2,1,0:T(8,1...) custom-call(bf16[168,2048]{1,0:T(8,128)(2,1)} %tok_ref.1, bf16[168,2048]{1,0:T(8,128)(2,1)} %cot_ref.1, ...), custom_call_target="tpu_custom_call" | custom-call | tf_op jit(solution)/shard_map/pallas_call | solution.py:911
  38.8 0.0 copy-done
  38.8 0.0 copy-done.1
  38.8 2.8 %shard_map.120 = (bf16[168,512]{1,0:T(8,128)(2,1)}, f32[2,168]{1,0:T(2,128)}, bf16[2,2048,256]{2,1,0:T(8,128)(2,1)}, bf16[2,2048,256]{2,1,0:T(8,128)(2,1)}, bf16[2,256,2048]{2,1,0:T(8,128)(2,1)}) custom-call(bf16[2,256,168]{2,1,0:T(8,128)(2,1)S(1)} %get-tuple-element.16.place_ref, bf16[256,512]{1,0:T(8,128)(2,1)S(1)} %get-tuple-element.17.back, ...), custom_call_target="tpu_custom_call" | custom-call | tf_op jit(solution)/shard_map/pallas_call | solution.py:927
Async XLA Ops:
  0.6 38.1 %copy-start = (s32[168,2]{0,1:T(2,128)S(1)}, s32[168,2]{0,1:T(2,128)}, u32[]{:S(2)}) copy-start(s32[168,2]{0,1:T(2,128)} %param.11) | copy-start | bytes 4036
  0.6 38.1 %copy-start.1 = (s32[168,1]{0,1:T(1,128)S(1)}, s32[168,1]{0,1:T(1,128)}, u32[]{:S(2)}) copy-start(s32[168,1]{0,1:T(1,128)} %param.10) | copy-start | bytes 2020

commit v2 on v1

--- a/solution.py
+++ b/solution.py
@@ -399,9 +399,9 @@
     tok_ref, cot_ref, gid_ref, wid_ref, gw_ref, wg_ref, wu_ref, wd_ref,
     place_ref, back, gate_back, vwg, vwu, vwd,
     gid, wid, gw, src, tok_all, cot_all, placed, rows_in, wg, wu, wd,
-    acc, gate_b, up_b, act_c, prod_hi, prod_lo, c_out, c_in,
+    wide, acc, gate_b, up_b, act_c, prod_hi, prod_lo, c_out, c_in,
     to_partner, from_partner, dx_acc, dx_far, to_x, from_x, to_ep, gate_in, gate_sum,
-    load_sem, send1, recv_rows, send_p, send_x, send_r, c_send, c_recv,
+    load_sem, wide_send, send1, recv_rows, send_p, send_x, send_r, c_send, c_recv,
     dxp_send, dxp_recv, dxx_send, dxx_recv, dxe_send, dxe_recv,
     gt_send, gt_recv, ge_send, ge_recv,
 ):
@@ -492,8 +492,21 @@
             device_id=(g, partner), device_id_type=MESH)
 
     others = list(range(1, ep))
-    for d in others[ep // 2 - 2::-1] + others[:ep // 2 - 2:-1]:
+    def send_wide():
+        return pltpu.make_async_remote_copy(
+            src_ref=wide, dst_ref=rows_in.at[beyond, block(e_me)],
+            send_sem=wide_send.at[0], recv_sem=recv_rows.at[beyond, e_me],
+            device_id=(xor(1), partner), device_id_type=MESH)
+
+    for d in others[1:ep // 2 - 1] + others[:1] + others[:ep // 2 - 2:-1]:
         send_rows(d).start()
+    loads[5].wait()
+    loads[6].wait()
+    beside = place_ref[0, block(xor(1)), :]
+    far_cols = pl.ds(pl.multiple_of(beyond * cs, LANES), cs)
+    wide[:, pl.ds(0, cs)] = dot(beside, tok_all[:, far_cols]).astype(bf16)
+    wide[:, pl.ds(cs, cs)] = dot(beside, cot_all[:, far_cols]).astype(bf16)
+    send_wide().start()
     lane_row = lax.broadcasted_iota(jnp.int32, (16, tok_rows), 0)
     weights = gw[...].astype(jnp.float32)
     comb = jnp.zeros((16, tok_rows), jnp.float32)
@@ -522,20 +535,26 @@
     def to_chips(ds):
         for d in ds:
             arrived(partner, d)
-            pass_on(partner, d, send_x, cross).start()
+            if d != 1:
+                pass_on(partner, d, send_x, cross).start()
             pass_on(partner, d, send_p, partner).start()
+
+    def relayed(d):
+        return pass_on(cross if d == 1 else beyond, d, send_r, partner)
 
     def relay(ds):
         for d in ds:
-            arrived(beyond, d)
-            pass_on(beyond, d, send_r, partner).start()
-
-    def wait_rows(q, ds):
+            arrived(cross if d == 1 else beyond, d)
+            relayed(d).start()
+
+    def wait_own(ds):
         for d in ds:
-            arrived(q, d)
-
-    loads[5].wait()
-    loads[6].wait()
+            arrived(t_me, d)
+
+    def wait_last(ds):
+        for d in ds:
+            arrived(beyond if d == 1 else cross, d)
+
     own = place_ref[0, block(e_me), :]
     own_x = dot(own, tok_all[...]).astype(bf16)
     own_y = dot(own, cot_all[...]).astype(bf16)
@@ -570,14 +589,22 @@
             out.append(values)
         return out
 
+    alone = pl.when(e_me >= 0)
+
+    def keep_half(chunk):
+        half(chunk, x_me, True)
+
     def first_half(chunk):
-        half(chunk, x_me, True)
+        alone(lambda: keep_half(chunk))
 
     lane = lax.broadcasted_iota(jnp.int32, (cap, lanes), 1)
     lane = lane - lax.broadcasted_iota(jnp.int32, (cap, lanes), 0)
     my_lane = lane == lax.rem(e_me * cap, lanes)
 
     def second_half(chunk):
+        alone(lambda: activations(chunk))
+
+    def activations(chunk):
         first, n, rows = chunk
         sums = half(chunk, x_other, False)
         for e in range(experts):
@@ -620,13 +647,22 @@
             device_id=(e_me, cross), device_id_type=MESH)
 
     def dx_first(i, chunk):
+        @alone
+        def _():
+            to_partner[0, chunk[2], :] = dx_of(chunk, cross, 1).astype(bf16)
+            dx_partner(0, i, chunk).start()
+
+    def dx_rest(i, chunk):
+        @alone
+        def _():
+            dx_other_chip(chunk)
+            dx_my_chip(i, chunk)
+
+    def dx_other_chip(chunk):
+        dx_far[chunk[2], :] = dx_of(chunk, beyond, 1)
+
+    def dx_my_chip(i, chunk):
         rows = chunk[2]
-        to_partner[0, rows, :] = dx_of(chunk, cross, 1).astype(bf16)
-        dx_partner(0, i, chunk).start()
-
-    def dx_rest(i, chunk):
-        rows = chunk[2]
-        dx_far[rows, :] = dx_of(chunk, beyond, 1)
         both = dx_of(chunk, 2 * x_me, 2)
         low, high = both[:, :cs], both[:, cs:]
         to_partner[1, rows, :] = jnp.where(core == 0, low, high).astype(bf16)
@@ -672,6 +708,9 @@
             device_id=(g, partner), device_id_type=MESH)
 
     def gates():
+        alone(gate_sums)
+
+    def gate_sums():
         row8 = lax.broadcasted_iota(jnp.int32, (8, slots), 0)
         ones = jnp.ones((8, prod_hi.shape[2]), bf16)
         value = jnp.zeros((8, slots), jnp.float32)
@@ -699,6 +738,9 @@
             gate_ep(d).start()
 
     def weight_grads(q):
+        alone(lambda: weight_quarter(q))
+
+    def weight_quarter(q):
         x_t = rows_in[q, :, pl.ds(0, cs)].T
         yq = rows_in[q, :, pl.ds(cs, cs)]
         for e in range(experts):
@@ -706,7 +748,7 @@
             vwu[e, share(q), :] = dot(x_t, up_b[e]).astype(bf16)
             vwd[e, :, share(q)] = dot(act_c[e], yq, TN).astype(bf16)
 
-    near = others[ep // 2 - 2::-1]
+    near = others[1:ep // 2 - 1] + others[:1]
     far_b = others[:-1 - ep // 4:-1]
     far_c = others[-1 - ep // 4:ep // 2 - 2:-1]
     far = far_b + far_c
@@ -723,11 +765,11 @@
     to_chips(near)
     for load in loads[7:]:
         load.wait()
-    wait_rows(t_me, near)
+    wait_own(near)
     first_half(a)
     to_chips(far_b)
-    relay(near)
-    wait_rows(cross, near)
+    relay(near[::-1])
+    wait_last(near)
     c_arrived(near)
     second_half(a)
     to_chips(far_c[:1])
@@ -735,31 +777,34 @@
     to_chips(far_c[1:])
     relay(far_b)
     dx_rest(0, a)
-    wait_rows(t_me, far)
+    wait_own(far)
     first_half(f)
-    wait_rows(cross, far_b)
+    dx_over(0, a, near + [0])
+    wait_last(far_b)
     c_arrived(far)
     second_half(b)
-    relay(far_c)
+    relay(far_c[:1])
     dx_first(1, b)
-    dx_rest(1, b)
+    alone(lambda: dx_other_chip(b))
+    relay(far_c[1:])
+    alone(lambda: dx_my_chip(1, b))
     dx_over(1, b, far_b)
-    dx_over(0, a, [0] + near)
-    wait_rows(cross, far_c)
+    own_ready(0, a)
+    wait_last(far_c)
     second_half(c)
     dx_first(2, c)
+    alone(lambda: dx_other_chip(c))
     gates()
-    dx_rest(2, c)
     dx_over(2, c, far_c)
+    alone(lambda: dx_my_chip(2, c))
     own_ready(1, b)
     send_back(far_b)
+    send_back(near + [0])
+    weight_grads(0)
     gates_on()
-    weight_grads(0)
-    own_ready(0, a)
     own_ready(2, c)
+    weight_grads(1)
     send_back(far_c)
-    send_back(near + [0])
-    weight_grads(1)
     weight_grads(2)
     weight_grads(3)
 
@@ -781,15 +826,17 @@
         returned(d)
     for d in range(ep):
         rows_back(d)
+    send_wide().wait_send()
     for d in range(ep):
         dx_x(d).wait_send()
         dx_ep(d).wait_send()
     for d in others:
         send_rows(d).wait_send()
         send_c(d).wait_send()
-        pass_on(partner, d, send_x, cross).wait_send()
+        if d != 1:
+            pass_on(partner, d, send_x, cross).wait_send()
         pass_on(partner, d, send_p, partner).wait_send()
-        pass_on(beyond, d, send_r, partner).wait_send()
+        relayed(d).wait_send()
         gate_ep(d).wait_send()
     for i, chunk in enumerate((a, b, c)):
         for k in range(2):
@@ -887,6 +934,7 @@
             pltpu.VMEM(w_gate.shape, bf16),
             pltpu.VMEM(w_up.shape, bf16),
             pltpu.VMEM(w_down.shape, bf16),
+            pltpu.VMEM((cap, 2 * cs), bf16),
             pltpu.VMEM((experts, 3, slots, ff), f32),
             pltpu.VMEM((experts, slots, ff), bf16),
             pltpu.VMEM((experts, slots, ff), bf16),
@@ -904,7 +952,7 @@
             pltpu.VMEM((slots, cs), bf16),
             pltpu.VMEM((tp, experts, slots), f32),
             pltpu.VMEM((slots // gate_lanes, experts, gate_lanes), f32),
-            dma((10,)), dma((ep,)), dma((tp, ep)), dma((ep,)), dma((ep,)), dma((ep,)),
+            dma((10,)), dma((1,)), dma((ep,)), dma((tp, ep)), dma((ep,)), dma((ep,)), dma((ep,)),
             dma((ep,)), dma((ep,)), dma((2, 3)), dma((2, 3)), dma((ep,)), dma((ep,)),
             dma((ep,)), dma((ep,)), dma((tp,)), dma((tp,)), dma((ep,)), dma((ep,)),
         ]

time: 41.8 us -> 39.5 us (0.945)
  Pallas kernels: 40.9 us -> 38.7 us
    pallas_call x1, Pallas kernels: 38.1 us -> 35.9 us  [on_device(): pl.pallas_call(functools.partial(body, ep, tp, cap), out_shape=(pltpu.VME...]
where the time goes in v2:
time: 39.5 us; the launch traced here: 39.4 us
  Pallas kernels  38.7 us (98%)
  between operations  0.67 us (2%)
    pallas_call x1, Pallas kernels, on_device(): pl.pallas_call(functools.partial(body, ep, tp, cap), out_shape=(pltpu.VME...  35.9 us
    pallas_call x1, Pallas kernels, on_device(): pl.pallas_call(finish, out_shape=(jax.ShapeDtypeStruct((tok_rows, cs), bf...  2.82 us

profile of v2, /device:TPU:0, one launch (start us, length us, event | category | flops | bytes accessed | tf_op | source)
XLA Modules:
  0.0 39.4 jit_solution(15573142378581537538)
XLA Ops:
  0.6 0.0 copy-start
  0.6 0.0 copy-start.1
  0.7 35.9 %shard_map.119 = (bf16[2,256,168]{2,1,0:T(8,128)(2,1)S(1)}, bf16[256,512]{1,0:T(8,128)(2,1)S(1)}, f32[8,2,128]{2,1,0:T(2,128)S(1)}, bf16[2,2048,256]{2,1,0:T(8,1...) custom-call(bf16[168,2048]{1,0:T(8,128)(2,1)} %tok_ref.1, bf16[168,2048]{1,0:T(8,128)(2,1)} %cot_ref.1, ...), custom_call_target="tpu_custom_call" | custom-call | tf_op jit(solution)/shard_map/pallas_call | solution.py:959
  36.5 0.0 copy-done
  36.6 0.0 copy-done.1
  36.6 2.8 %shard_map.120 = (bf16[168,512]{1,0:T(8,128)(2,1)}, f32[2,168]{1,0:T(2,128)}, bf16[2,2048,256]{2,1,0:T(8,128)(2,1)}, bf16[2,2048,256]{2,1,0:T(8,128)(2,1)}, bf16[2,256,2048]{2,1,0:T(8,128)(2,1)}) custom-call(bf16[2,256,168]{2,1,0:T(8,128)(2,1)S(1)} %get-tuple-element.16.place_ref, bf16[256,512]{1,0:T(8,128)(2,1)S(1)} %get-tuple-element.17.back, ...), custom_call_target="tpu_custom_call" | custom-call | tf_op jit(solution)/shard_map/pallas_call | solution.py:975
Async XLA Ops:
  0.6 35.9 %copy-start = (s32[168,2]{0,1:T(2,128)S(1)}, s32[168,2]{0,1:T(2,128)}, u32[]{:S(2)}) copy-start(s32[168,2]{0,1:T(2,128)} %param.11) | copy-start | bytes 4036
  0.6 35.9 %copy-start.1 = (s32[168,1]{0,1:T(1,128)S(1)}, s32[168,1]{0,1:T(1,128)}, u32[]{:S(2)}) copy-start(s32[168,1]{0,1:T(1,128)} %param.10) | copy-start | bytes 2020

commit v3 on v2

--- a/solution.py
+++ b/solution.py
@@ -498,15 +498,8 @@
             send_sem=wide_send.at[0], recv_sem=recv_rows.at[beyond, e_me],
             device_id=(xor(1), partner), device_id_type=MESH)
 
-    for d in others[1:ep // 2 - 1] + others[:1] + others[:ep // 2 - 2:-1]:
+    for d in others[1:ep // 2 - 1] + others[:1]:
         send_rows(d).start()
-    loads[5].wait()
-    loads[6].wait()
-    beside = place_ref[0, block(xor(1)), :]
-    far_cols = pl.ds(pl.multiple_of(beyond * cs, LANES), cs)
-    wide[:, pl.ds(0, cs)] = dot(beside, tok_all[:, far_cols]).astype(bf16)
-    wide[:, pl.ds(cs, cs)] = dot(beside, cot_all[:, far_cols]).astype(bf16)
-    send_wide().start()
     lane_row = lax.broadcasted_iota(jnp.int32, (16, tok_rows), 0)
     weights = gw[...].astype(jnp.float32)
     comb = jnp.zeros((16, tok_rows), jnp.float32)
@@ -515,8 +508,19 @@
     c_rows = dot(comb.astype(bf16), place, NT)
     for i in range(slots // lanes):
         c_out[i] = c_rows[:experts, i * lanes : (i + 1) * lanes]
-    for d in others:
+    for d in others[:ep // 2 - 1]:
         send_c(d).start()
+    for d in others[:ep // 2 - 2:-1]:
+        send_rows(d).start()
+    for d in others[ep // 2 - 1:]:
+        send_c(d).start()
+    loads[5].wait()
+    loads[6].wait()
+    beside = place_ref[0, block(xor(1)), :]
+    far_cols = pl.ds(pl.multiple_of(beyond * cs, LANES), cs)
+    wide[:, pl.ds(0, cs)] = dot(beside, tok_all[:, far_cols]).astype(bf16)
+    wide[:, pl.ds(cs, cs)] = dot(beside, cot_all[:, far_cols]).astype(bf16)
+    send_wide().start()
 
     def arrived(q, d):
         e = xor(d)
@@ -671,6 +675,9 @@
 
     def dx_over(i, chunk, ds):
         dx_partner(0, i, chunk).wait_recv()
+        dx_send(ds)
+
+    def dx_send(ds):
         for d in ds:
             rows = block(xor(d))
             to_x[rows, :] = (dx_far[rows, :] + from_partner[0, rows, :].astype(jnp.float32)).astype(bf16)
@@ -779,7 +786,8 @@
     dx_rest(0, a)
     wait_own(far)
     first_half(f)
-    dx_over(0, a, near + [0])
+    dx_partner(0, 0, a).wait_recv()
+    dx_send(near[:-1])
     wait_last(far_b)
     c_arrived(far)
     second_half(b)
@@ -796,15 +804,17 @@
     alone(lambda: dx_other_chip(c))
     gates()
     dx_over(2, c, far_c)
-    alone(lambda: dx_my_chip(2, c))
+    dx_send(near[-1:] + [0])
     own_ready(1, b)
     send_back(far_b)
-    send_back(near + [0])
+    alone(lambda: dx_my_chip(2, c))
+    send_back(near[:-1])
     weight_grads(0)
     gates_on()
     own_ready(2, c)
     weight_grads(1)
     send_back(far_c)
+    send_back(near[-1:] + [0])
     weight_grads(2)
     weight_grads(3)
 

time: 39.5 us -> 39.3 us (level)
  no operation moved by 1% of the time
where the time goes in v3:
time: 39.3 us; the launch traced here: 39.1 us
  Pallas kernels  38.4 us (98%)
  between operations  0.67 us (2%)
    pallas_call x1, Pallas kernels, on_device(): pl.pallas_call(functools.partial(body, ep, tp, cap), out_shape=(pltpu.VME...  35.6 us
    pallas_call x1, Pallas kernels, on_device(): pl.pallas_call(finish, out_shape=(jax.ShapeDtypeStruct((tok_rows, cs), bf...  2.82 us

profile of v3, /device:TPU:0, one launch (start us, length us, event | category | flops | bytes accessed | tf_op | source)
XLA Modules:
  0.0 39.1 jit_solution(10230647320864561973)
XLA Ops:
  0.6 0.0 copy-start
  0.6 0.0 copy-start.1
  0.7 35.6 %shard_map.119 = (bf16[2,256,168]{2,1,0:T(8,128)(2,1)S(1)}, bf16[256,512]{1,0:T(8,128)(2,1)S(1)}, f32[8,2,128]{2,1,0:T(2,128)S(1)}, bf16[2,2048,256]{2,1,0:T(8,1...) custom-call(bf16[168,2048]{1,0:T(8,128)(2,1)} %tok_ref.1, bf16[168,2048]{1,0:T(8,128)(2,1)} %cot_ref.1, ...), custom_call_target="tpu_custom_call" | custom-call | tf_op jit(solution)/shard_map/pallas_call | solution.py:969
  36.3 0.0 copy-done
  36.3 0.0 copy-done.1
  36.3 2.8 %shard_map.120 = (bf16[168,512]{1,0:T(8,128)(2,1)}, f32[2,168]{1,0:T(2,128)}, bf16[2,2048,256]{2,1,0:T(8,128)(2,1)}, bf16[2,2048,256]{2,1,0:T(8,128)(2,1)}, bf16[2,256,2048]{2,1,0:T(8,128)(2,1)}) custom-call(bf16[2,256,168]{2,1,0:T(8,128)(2,1)S(1)} %get-tuple-element.16.place_ref, bf16[256,512]{1,0:T(8,128)(2,1)S(1)} %get-tuple-element.17.back, ...), custom_call_target="tpu_custom_call" | custom-call | tf_op jit(solution)/shard_map/pallas_call | solution.py:985
Async XLA Ops:
  0.6 35.6 %copy-start = (s32[168,2]{0,1:T(2,128)S(1)}, s32[168,2]{0,1:T(2,128)}, u32[]{:S(2)}) copy-start(s32[168,2]{0,1:T(2,128)} %param.11) | copy-start | bytes 4036
  0.6 35.6 %copy-start.1 = (s32[168,1]{0,1:T(1,128)S(1)}, s32[168,1]{0,1:T(1,128)}, u32[]{:S(2)}) copy-start(s32[168,1]{0,1:T(1,128)} %param.10) | copy-start | bytes 2020
